TPU v7x, 32 devices: a whole 2x2x4 slice. The times are simulated.
32 devices in a mesh: ep: 16 (over z, x, core), tp: 2 (over y).
Axes of the slice: x: 2, y: 2, z: 4, core: 2. Of those that a mesh axis runs over, the one named last changes fastest.
Arguments:
- tokens: bfloat16 [2048, 2048], P('ep'), may hold values from -6 to 6
- cotangent: bfloat16 [2048, 2048], P('ep'), may hold values from -1.796875 to 1.796875
- group_weight: float32 [2048], P('ep'), may hold values from 0.2 to 1
- expert_weight: float32 [2048, 2], P('ep'), may hold values from 0.1 to 0.9
- group_choice: int32 [2048], P('ep'), may hold values from 0 to 3, as said below
- local_choice: int32 [2048, 2], P('ep'), may hold values from 0 to 3, as said below
- w_gate: bfloat16 [16, 2048, 512], P('ep', None, 'tp'), may hold values from -0.125 to 0.125
- w_up: bfloat16 [16, 2048, 512], P('ep', None, 'tp'), may hold values from -0.125 to 0.125
- w_down: bfloat16 [16, 512, 2048], P('ep', 'tp'), may hold values from -0.25 to 0.25
Outputs:
- token_grad: float32 [2048, 2048], P('ep', 'tp')
- group_weight_grad: float32 [2048], P('ep')
- expert_weight_grad: float32 [2048, 2], P('ep')
- w_gate_grad: float32 [16, 2048, 512], P('ep', None, 'tp')
- w_up_grad: float32 [16, 2048, 512], P('ep', None, 'tp')
- w_down_grad: float32 [16, 512, 2048], P('ep', 'tp')
Inputs may be any that keep to these rules, and one draw needn't show every extreme that they name: Among the 128 tokens of each device (aligned blocks of tokens), no expert 4 * group_choice + local_choice is named by more than 24 slots, and some expert is named by exactly 24 slots of every device. `local_choice`: the 2 local choices of a token differ.
All inputs are finite; a program needn't handle non-finite values.
Results may differ from a plain program's by a relative error of at most 0.006.
Values may be sent and summed in bfloat16 or wider, within the bound.
A program may use at most 64 MiB of HBM per device.

v0:
```python
import jax
import jax.numpy as jnp
from jax import lax
from jax.sharding import PartitionSpec as P

EPG = 4


def shards(
    tokens, cotangent, group_weight, expert_weight, group_choice, local_choice, w_gate, w_up, w_down
):
    token_count, feature_count = tokens.shape
    pick_count = expert_weight.shape[1]
    expert_count = lax.axis_size("ep")
    lane_count = lax.axis_size("tp")
    slot_count = token_count * pick_count
    capacity = pick_count * (3 * token_count // (2 * expert_count))
    buffer_count = expert_count * capacity
    piece_width = feature_count // lane_count
    expert_of = (group_choice[:, None] * EPG + local_choice).reshape(slot_count)
    member = (expert_of[:, None] == jnp.arange(expert_count, dtype=jnp.int32)[None, :]).astype(
        jnp.bfloat16
    )
    order = jnp.arange(slot_count, dtype=jnp.int32)
    earlier_mask = (order[:, None] > order[None, :]).astype(jnp.bfloat16)
    earlier = jnp.dot(earlier_mask, member, preferred_element_type=jnp.float32)
    position = jnp.sum(earlier * member.astype(jnp.float32), axis=1).astype(jnp.int32)
    slot_index = expert_of * capacity + position
    owner = (
        jnp.full((buffer_count,), token_count, jnp.int32).at[slot_index].set(order // pick_count)
    )
    gate_value = (group_weight[:, None] * expert_weight).astype(jnp.bfloat16).reshape(slot_count)
    gate_buffer = jnp.zeros((buffer_count,), jnp.bfloat16).at[slot_index].set(gate_value)
    start = lax.axis_index("tp") * piece_width
    token_cols = lax.dynamic_slice_in_dim(tokens, start, piece_width, 1)
    cot_cols = lax.dynamic_slice_in_dim(cotangent, start, piece_width, 1)
    token_part = jnp.take(token_cols, owner, axis=0, mode="fill", fill_value=0)
    cot_part = jnp.take(cot_cols, owner, axis=0, mode="fill", fill_value=0)
    token_part, gate_rows, cot_part = (
        lax.all_to_all(token_part, "ep", split_axis=0, concat_axis=0, tiled=True),
        lax.all_to_all(gate_buffer, "ep", split_axis=0, concat_axis=0, tiled=True),
        lax.all_to_all(cot_part, "ep", split_axis=0, concat_axis=0, tiled=True),
    )
    arrived, cot_rows = (
        lax.all_gather(token_part, "tp", axis=1, tiled=True),
        lax.all_gather(cot_part, "tp", axis=1, tiled=True),
    )
    first = w_gate[0]
    second = w_up[0]
    third = w_down[0]
    contract_cols = (((1,), (1,)), ((), ()))
    contract_rows = (((0,), (0,)), ((), ()))
    pre_gate = jnp.dot(arrived, first, preferred_element_type=jnp.float32)
    pre_up = jnp.dot(arrived, second, preferred_element_type=jnp.float32)
    back_hidden = lax.dot_general(
        cot_rows, third, contract_cols, preferred_element_type=jnp.float32
    )
    sigma = jax.nn.sigmoid(pre_gate)
    swish = pre_gate * sigma
    hidden = swish * pre_up
    gate_part = jnp.sum(hidden * back_hidden, axis=1)
    gate_float = gate_rows.reshape(buffer_count, 1).astype(jnp.float32)
    scaled = gate_float * back_hidden
    grad_gate_pre = (scaled * pre_up * sigma * (1.0 + pre_gate * (1.0 - sigma))).astype(
        jnp.bfloat16
    )
    grad_up_pre = (scaled * swish).astype(jnp.bfloat16)
    weighted = (gate_float * hidden).astype(jnp.bfloat16)
    first_grad = lax.dot_general(
        arrived, grad_gate_pre, contract_rows, preferred_element_type=jnp.float32
    )
    second_grad = lax.dot_general(
        arrived, grad_up_pre, contract_rows, preferred_element_type=jnp.float32
    )
    third_grad = lax.dot_general(
        weighted, cot_rows, contract_rows, preferred_element_type=jnp.float32
    )
    partial_value = lax.dot_general(
        grad_gate_pre, first, contract_cols, preferred_element_type=jnp.float32
    )
    partial_value = partial_value + lax.dot_general(
        grad_up_pre, second, contract_cols, preferred_element_type=jnp.float32
    )
    pieces = lax.all_to_all(partial_value, "tp", split_axis=1, concat_axis=0, tiled=True)
    row_grad = jnp.sum(pieces.reshape(lane_count, buffer_count, piece_width), axis=0).astype(
        jnp.bfloat16
    )
    gate_total = lax.psum(gate_part, "tp").astype(jnp.bfloat16)
    returned, gate_back = (
        lax.all_to_all(row_grad, "ep", split_axis=0, concat_axis=0, tiled=True),
        lax.all_to_all(gate_total, "ep", split_axis=0, concat_axis=0, tiled=True),
    )
    slot_grad = jnp.take(returned, slot_index, axis=0).astype(jnp.float32)
    token_grad = jnp.sum(slot_grad.reshape(token_count, pick_count, piece_width), axis=1)
    gate_grad = (
        jnp.take(gate_back, slot_index, axis=0).astype(jnp.float32).reshape(token_count, pick_count)
    )
    group_grad = jnp.sum(expert_weight * gate_grad, axis=1)
    expert_grad = group_weight[:, None] * gate_grad
    return (
        token_grad,
        group_grad,
        expert_grad,
        first_grad[None],
        second_grad[None],
        third_grad[None],
    )


def solution(mesh):
    in_specs = (
        P("ep", None),
        P("ep", None),
        P("ep"),
        P("ep", None),
        P("ep"),
        P("ep", None),
        P("ep", None, "tp"),
        P("ep", None, "tp"),
        P("ep", "tp", None),
    )
    out_specs = (
        P("ep", "tp"),
        P("ep"),
        P("ep", None),
        P("ep", None, "tp"),
        P("ep", None, "tp"),
        P("ep", "tp", None),
    )
    return jax.shard_map(shards, mesh=mesh, in_specs=in_specs, out_specs=out_specs, check_vma=False)
```

profile of v0, /device:TPU:0, one launch (start us, length us, event | category | flops | bytes accessed | tf_op | source)
XLA Modules:
  0.0 192.5 jit_solution(5820197067806515921)
XLA Ops:
  7.2 0.9 copy.21
  8.1 0.7 broadcast_multiply_fusion.2
  8.8 0.1 reshape.103
  9.0 0.2 fusion
  9.2 0.1 mul.93
  9.4 1.4 scatter_custom_fusion.1
  10.8 1.1 constant_dynamic-slice_fusion
  11.9 2.1 %gather_fusion.3 = bf16[384,1024]{1,0:T(8,128)(2,1)S(1)} fusion(bf16[128,1024]{1,0:T(8,128)(2,1)S(1)} %get-tuple-element.28, s32[1024]{0:T(1024)S(1)} %pad_clamp_fusion.1), kind=kCustom, calls=%fused_computation.1.clone | custom fusion | bytes 1574400 | tf_op jit(solution)/shard_map/jit(_take)/gather | solution.py:37
  14.0 2.1 %gather_fusion.2 = bf16[384,1024]{1,0:T(8,128)(2,1)S(1)} fusion(bf16[128,1024]{1,0:T(8,128)(2,1)S(1)} %get-tuple-element.29, s32[1024]{0:T(1024)S(1)} %pad_clamp_fusion.1), kind=kCustom, calls=%fused_computation.clone | custom fusion | bytes 1574400 | tf_op jit(solution)/shard_map/jit(_take)/gather | solution.py:38
  16.1 0.2 broadcast_select_fusion.2
  16.2 27.4 %all_to_all.69 = bf16[16,24,1024]{2,1,0:T(8,128)(2,1)} all-to-all(bf16[16,24,1024]{2,1,0:T(8,128)(2,1)S(1)} %bitcast.50), channel_id=1, replica_groups=mesh['ep'=16,'tp'=2] {'ep'}, dimensions={0} | all-to-all | bytes 1572864 | tf_op jit(solution)/shard_map/all_to_all | solution.py:40
  43.7 24.0 %all_to_all.70 = bf16[16,24,1024]{2,1,0:T(8,128)(2,1)} all-to-all(bf16[16,24,1024]{2,1,0:T(8,128)(2,1)S(1)} %bitcast.49), channel_id=1, replica_groups=mesh['ep'=16,'tp'=2] {'ep'}, dimensions={0} | all-to-all | bytes 1572864 | tf_op jit(solution)/shard_map/all_to_all | solution.py:42
  67.7 0.1 copy.23
  67.9 0.1 reshape.142
  68.0 2.2 %scatter_custom_fusion = bf16[384]{0:T(512)(128)(2,1)S(1)} fusion(s32[256]{0:T(256)S(1)} %bitcast.53, bf16[256]{0:T(256)(128)(2,1)S(1)} %reshape.142, bf16[]{:T(256)} %constant.47.clone.1), kind=kCustom, calls=%fused_computation.58 | custom fusion | bytes 770 | tf_op jit(solution)/shard_map/scatter | solution.py:33
  70.2 0.1 all_to_all.61
  70.3 10.2 %all_to_all.71 = bf16[16,24,1]{1,2,0:T(2,128)(2,1)S(1)} all-to-all(bf16[16,24,1]{1,2,0:T(2,128)(2,1)S(1)} %all_to_all.61), channel_id=1, replica_groups=mesh['ep'=16,'tp'=2] {'ep'}, dimensions={0} | all-to-all | bytes 1536 | tf_op jit(solution)/shard_map/all_to_all | solution.py:41
  80.6 2.3 %fusion.3 = f32[384,256]{0,1:T(8,128)S(1)} fusion(bf16[384,2048]{1,0:T(8,128)(2,1)} %all-gather.5.cloned.1.call-done, bf16[1,2048,256]{2,1,0:T(8,128)(2,1)S(1)} %copy-done), kind=kOutput, calls=%fused_computation.15 | convolution fusion | flops 402653184 | bytes 3014656 | tf_op jit(solution)/shard_map/dot_general | solution.py:53
  82.9 2.1 %fusion.6 = f32[384,256]{0,1:T(8,128)S(1)} fusion(bf16[384,2048]{1,0:T(8,128)(2,1)S(1)} %copy-done.1, bf16[1,2048,256]{2,1,0:T(8,128)(2,1)} %param.18), kind=kOutput, calls=%fused_computation.18 | convolution fusion | flops 402653184 | bytes 3014656 | tf_op jit(solution)/shard_map/dot_general | solution.py:54
  85.1 14.0 %all-gather.3.cloned.1.call-done = bf16[384,2048]{1,0:T(8,128)(2,1)} async-done(((bf16[384,1024]{1,0:T(8,128)(2,1)}), bf16[384,2048]{1,0:T(8,128)(2,1)}) %all-gather.3.cloned.1.call-update) | async-done | bytes 1572880 | tf_op jit(solution)/shard_map/all_gather | solution.py:46
  99.1 2.5 %multiply_reduce_fusion = (f32[384]{0:T(512)S(1)}, bf16[384,256]{0,1:T(8,128)(2,1)S(1)}, bf16[384,256]{0,1:T(8,128)(2,1)S(1)}) fusion(f32[384,256]{0,1:T(8,128)S(1)} %fusion.6, f32[384,256]{0,1:T(8,128)S(1)} %fusion.3, f32[384]{0:T(512)S(1)} %reshape.105, bf16[384,2048]{1,0:T(8,128)(2,1)} %all-gather.3.cloned.1.call-done, bf16[1,256,2048]{2,1,0:T(8,128)(2,1)} %param.19), kind=kOutput, calls=%fused_computation.27 | convolution fusion | flops 404323968 | bytes 3804160 | tf_op jit(solution)/shard_map/dot_general | solution.py:55
  101.7 0.6 fusion.1
  102.4 0.6 copy-done.2
  103.0 0.6 convolution_add_fusion
  103.7 1.9 copy.31
  105.6 5.2 %all-to-all-start.3 = ((f32[384,2,1024]{2,0,1:T(8,128)}), f32[384,2,1024]{2,0,1:T(8,128)}, u32[]{:S(2)}, u32[]{:S(2)}) async-start(f32[384,2,1024]{2,0,1:T(8,128)} %bitcast.45), calls=%async_computation.3 | async-start | bytes 6291456 | tf_op jit(solution)/shard_map/all_to_all | solution.py:84
  110.8 36.3 %psum.7 = bf16[384]{0:T(512)(128)(2,1)S(1)} all-reduce(f32[384]{0:T(512)S(1)} %get-tuple-element.23), channel_id=1, replica_groups=mesh['ep'=16,'tp'=2] {'tp'}, use_global_device_ids=true, to_apply=%region_6.8 | all-reduce | flops 384 | bytes 2304 | tf_op jit(solution)/shard_map/psum | solution.py:88
  147.1 0.7 all_to_all.62
  147.8 5.6 %all-to-all-start.5 = ((bf16[16,24,1]{1,2,0:T(2,128)(2,1)}), bf16[16,24,1]{1,2,0:T(2,128)(2,1)S(1)}, u32[]{:S(2)}, u32[]{:S(2)}) async-start(bf16[16,24,1]{1,2,0:T(2,128)(2,1)} %all_to_all.62), calls=%async_computation.5 | async-start | bytes 16384 | tf_op jit(solution)/shard_map/all_to_all | solution.py:91
  153.4 3.3 %reduce_sum.46 = bf16[384,1024]{1,0:T(8,128)(2,1)} reduce(f32[384,2,1024]{2,0,1:T(8,128)} %all-to-all-done.3, f32[]{:T(128)} %constant.43.clone.1), dimensions={1}, to_apply=%region_3.5 | reduce | flops 393216 | bytes 3932164 | tf_op jit(solution)/shard_map/reduce_sum | solution.py:85
  156.7 3.1 %all-to-all-done.5 = bf16[16,24,1]{1,2,0:T(2,128)(2,1)S(1)} async-done(((bf16[16,24,1]{1,2,0:T(2,128)(2,1)}), bf16[16,24,1]{1,2,0:T(2,128)(2,1)S(1)}, u32[]{:S(2)}, u32[]{:S(2)}) %all-to-all-start.5) | async-done | bytes 800 | tf_op jit(solution)/shard_map/all_to_all | solution.py:91
  159.8 3.8 %all-to-all-start.4 = ((bf16[16,24,1024]{2,1,0:T(8,128)(2,1)}), bf16[16,24,1024]{2,1,0:T(8,128)(2,1)S(1)}, u32[]{:S(2)}, u32[]{:S(2)}) async-start(bf16[16,24,1024]{2,1,0:T(8,128)(2,1)} %bitcast.48), calls=%async_computation.4 | async-start | bytes 1572864 | tf_op jit(solution)/shard_map/all_to_all | solution.py:90
  163.6 0.8 convert_element_type.71
  164.3 0.1 copy.27
  164.5 0.7 pad_clamp_fusion
  165.1 3.0 %convolution_bitcast_fusion.1 = f32[1,2048,256]{2,1,0:T(8,128)} fusion(bf16[384,2048]{1,0:T(8,128)(2,1)S(1)} %copy-done.1, bf16[384,256]{0,1:T(8,128)(2,1)} %copy-done.10), kind=kOutput, calls=%fused_computation.9 | convolution fusion | flops 402653184 | bytes 3866624 | tf_op jit(solution)/shard_map/dot_general | solution.py:72
  168.2 2.1 %convolution_bitcast_fusion.2 = f32[1,2048,256]{2,1,0:T(8,128)} fusion(bf16[384,2048]{1,0:T(8,128)(2,1)S(1)} %copy-done.1, bf16[384,256]{0,1:T(8,128)(2,1)S(1)} %copy-done.9), kind=kOutput, calls=%fused_computation.10 | convolution fusion | flops 402653184 | bytes 3866624 | tf_op jit(solution)/shard_map/dot_general | solution.py:69
  170.3 2.1 %convolution_bitcast_fusion = f32[1,256,2048]{2,1,0:T(8,128)} fusion(bf16[384,2048]{1,0:T(8,128)(2,1)S(1)} %copy-done.3, f32[384]{0:T(512)S(1)} %reshape.105, f32[384,256]{0,1:T(8,128)S(1)} %copy-done.7, f32[384,256]{0,1:T(8,128)S(1)} %copy-done.5), kind=kOutput, calls=%fused_computation.8 | convolution fusion | flops 403341312 | bytes 4457984 | tf_op jit(solution)/shard_map/dot_general | solution.py:75
  172.4 0.1 all_to_all.60
  172.5 1.9 %gather_fusion.1 = bf16[256]{0:T(256)(128)(2,1)S(1)} fusion(bf16[384]{0:T(512)(128)(2,1)S(1)} %all_to_all.60, s32[1024]{0:T(1024)S(1)} %pad_clamp_fusion), kind=kCustom, calls=%fused_computation.3 | custom fusion | bytes 2048 | tf_op jit(solution)/shard_map/jit(_take)/gather | solution.py:96
  174.4 0.2 gather.18
  174.6 0.1 convert_multiply_fusion
  174.7 0.6 copy.28
  175.3 0.6 fusion.13
  176.0 6.1 %all-to-all-done.4 = bf16[16,24,1024]{2,1,0:T(8,128)(2,1)S(1)} async-done(((bf16[16,24,1024]{2,1,0:T(8,128)(2,1)}), bf16[16,24,1024]{2,1,0:T(8,128)(2,1)S(1)}, u32[]{:S(2)}, u32[]{:S(2)}) %all-to-all-start.4) | async-done | bytes 786464 | tf_op jit(solution)/shard_map/all_to_all | solution.py:90
  182.0 1.2 gather_fusion
  183.2 0.2 gather.16
  183.4 2.2 %convert_reduce_fusion = f32[128,1024]{1,0:T(8,128)} fusion(bf16[128,2,1024]{2,1,0:T(2,128)(2,1)S(1)} %gather.16, pred[128,2]{1,0:T(8,128)(4,1)S(1)} %get-tuple-element.20), kind=kLoop, calls=%fused_computation.22 | loop fusion | flops 655360 | bytes 1048832 | tf_op jit(solution)/shard_map/reduce_sum | solution.py:94
  (48 shorter events, 0.6 us)
Async XLA Ops:
  7.2 73.5 %copy-start = (bf16[1,2048,256]{2,1,0:T(8,128)(2,1)S(1)}, bf16[1,2048,256]{2,1,0:T(8,128)(2,1)}, u32[]{:S(2)}) copy-start(bf16[1,2048,256]{2,1,0:T(8,128)(2,1)} %param.17) | copy-start | bytes 3145732
  7.2 73.4 %all-gather.5.cloned.1.call-start = ((), (), s32[]{:S(2)}) async-start(), calls=%async_computation.7 | async-start | bytes 2359296 | tf_op jit(solution)/shard_map/all_gather | solution.py:45
  9.4 58.7 %copy-start.13 = (s32[256,1]{0,1:T(1,128)}, s32[256,1]{0,1:T(1,128)S(1)}, u32[]{:S(2)}) copy-start(s32[256,1]{0,1:T(1,128)S(1)} %compare_select_fusion.1) | copy-start | bytes 3076
  43.6 24.1 %copy-start.12 = (f32[128,2]{0,1:T(2,128)S(1)}, f32[128,2]{0,1:T(2,128)}, u32[]{:S(2)}) copy-start(f32[128,2]{0,1:T(2,128)} %param.14) | copy-start | bytes 3076
  43.6 24.1 %copy-start.14 = (f32[128]{0:T(128)S(1)}, f32[128]{0:T(128)}, u32[]{:S(2)}) copy-start(f32[128]{0:T(128)} %param.13) | copy-start | bytes 1540
  43.7 55.4 %all-gather.3.cloned.1.call-start = ((), (), s32[]{:S(2)}) async-start(), calls=%async_computation.6 | async-start | bytes 2359296 | tf_op jit(solution)/shard_map/all_gather | solution.py:46
  80.6 2.3 %copy-start.1 = (bf16[384,2048]{1,0:T(8,128)(2,1)S(1)}, bf16[384,2048]{1,0:T(8,128)(2,1)}, u32[]{:S(2)}) copy-start(bf16[384,2048]{1,0:T(8,128)(2,1)} %all-gather.5.cloned.1.call-done) | copy-start | bytes 4718596
  82.9 18.7 %copy-start.4 = (f32[384,256]{0,1:T(8,128)}, f32[384,256]{0,1:T(8,128)S(1)}, u32[]{:S(2)}) copy-start(f32[384,256]{0,1:T(8,128)S(1)} %fusion.3) | copy-start | bytes 1179652
  85.1 16.6 %copy-start.6 = (f32[384,256]{0,1:T(8,128)}, f32[384,256]{0,1:T(8,128)S(1)}, u32[]{:S(2)}) copy-start(f32[384,256]{0,1:T(8,128)S(1)} %fusion.6) | copy-start | bytes 1179652
  101.6 0.7 copy-start.8
  101.7 0.7 copy-start.10
  101.7 1.4 copy-start.2
  105.6 42.2 %all-to-all-start.3 = ((f32[384,2,1024]{2,0,1:T(8,128)}), f32[384,2,1024]{2,0,1:T(8,128)}, u32[]{:S(2)}, u32[]{:S(2)}) async-start(f32[384,2,1024]{2,0,1:T(8,128)} %bitcast.45), calls=%async_computation.3 | async-start | bytes 6291456 | tf_op jit(solution)/shard_map/all_to_all | solution.py:84
  147.8 12.0 %all-to-all-start.5 = ((bf16[16,24,1]{1,2,0:T(2,128)(2,1)}), bf16[16,24,1]{1,2,0:T(2,128)(2,1)S(1)}, u32[]{:S(2)}, u32[]{:S(2)}) async-start(bf16[16,24,1]{1,2,0:T(2,128)(2,1)} %all_to_all.62), calls=%async_computation.5 | async-start | bytes 16384 | tf_op jit(solution)/shard_map/all_to_all | solution.py:91
  159.8 22.3 %all-to-all-start.4 = ((bf16[16,24,1024]{2,1,0:T(8,128)(2,1)}), bf16[16,24,1024]{2,1,0:T(8,128)(2,1)S(1)}, u32[]{:S(2)}, u32[]{:S(2)}) async-start(bf16[16,24,1024]{2,1,0:T(8,128)(2,1)} %bitcast.48), calls=%async_computation.4 | async-start | bytes 1572864 | tf_op jit(solution)/shard_map/all_to_all | solution.py:90
  165.1 3.0 %copy-start.9 = (bf16[384,256]{0,1:T(8,128)(2,1)S(1)}, bf16[384,256]{0,1:T(8,128)(2,1)}, u32[]{:S(2)}) copy-start(bf16[384,256]{0,1:T(8,128)(2,1)} %copy-done.8) | copy-start | bytes 589828
  168.2 2.1 %copy-start.3 = (bf16[384,2048]{1,0:T(8,128)(2,1)S(1)}, bf16[384,2048]{1,0:T(8,128)(2,1)}, u32[]{:S(2)}) copy-start(bf16[384,2048]{1,0:T(8,128)(2,1)} %all-gather.3.cloned.1.call-done) | copy-start | bytes 4718596
  168.2 2.1 %copy-start.5 = (f32[384,256]{0,1:T(8,128)S(1)}, f32[384,256]{0,1:T(8,128)}, u32[]{:S(2)}) copy-start(f32[384,256]{0,1:T(8,128)} %copy-done.4) | copy-start | bytes 1179652
  168.2 2.1 %copy-start.7 = (f32[384,256]{0,1:T(8,128)S(1)}, f32[384,256]{0,1:T(8,128)}, u32[]{:S(2)}) copy-start(f32[384,256]{0,1:T(8,128)} %copy-done.6) | copy-start | bytes 1179652
  170.3 4.3 %copy-start.11 = (s32[128,2]{1,0:T(8,128)S(1)}, s32[128,2]{1,0:T(8,128)}, u32[]{:S(2)}) copy-start(s32[128,2]{1,0:T(8,128)} %convert_element_type.71) | copy-start | bytes 3076
  170.3 4.3 %copy-start.15 = (f32[128]{0:T(128)S(1)}, f32[128]{0:T(128)}, u32[]{:S(2)}) copy-start(f32[128]{0:T(128)} %param.13) | copy-start | bytes 1540
Sparse Core Ops, SparseCore 0:
  43.8 26.4 all-gather.4
  71.9 27.1 all-gather.2
where the time goes:
time: 193 us; the launch traced here: 192 us
  blocking collectives  97.9 us (51%)
  waiting for transfers between devices  23.2 us (12%)
  local copies, waits for them, and re-layouts  18.8 us (10%)
  matrix products  15.6 us (8%)
  starting transfers between devices  14.7 us (8%)
  between operations  14.4 us (7%)
  other arithmetic  7.91 us (4%)
    psum x1, blocking collectives, shards(): gate_total = lax.psum(gate_part, 'tp').astype(jnp.bfloat16)  36.3 us
    all_to_all x1, blocking collectives, shards(): lax.all_to_all(token_part, 'ep', split_axis=0, concat_axis=0, tiled=True)  27.4 us
    all_to_all x1, blocking collectives, shards(): lax.all_to_all(cot_part, 'ep', split_axis=0, concat_axis=0, tiled=True)  24 us
    all_gather x1, waiting for transfers between devices, shards(): lax.all_gather(cot_part, 'tp', axis=1, tiled=True)  14 us
    all_to_all x1, blocking collectives, shards(): lax.all_to_all(gate_buffer, 'ep', split_axis=0, concat_axis=0, tiled=True)  10.2 us
    all_to_all x1, waiting for transfers between devices, shards(): lax.all_to_all(row_grad, 'ep', split_axis=0, concat_axis=0, tiled=True)  6.06 us
    all_to_all x1, starting transfers between devices, shards(): lax.all_to_all(gate_total, 'ep', split_axis=0, concat_axis=0, tiled=True)  5.61 us
    all_to_all x1, starting transfers between devices, shards(): lax.all_to_all(partial_value, 'tp', split_axis=1, concat_axis=0, tiled=True)  5.21 us
  transfers between devices with their start and end apart: 5, of which 3 were waited for; matrix products, arithmetic and copies ran while one was open for 12% of the time, Pallas kernels for 0%

commit v1 on v0

v1 whole, which is shorter than its diff:
```python
import jax
import jax.numpy as jnp
from jax import lax
from jax.sharding import Mesh, PartitionSpec as P

EPG = 4
LANES = 128


def shards(
    tokens, cotangent, group_weight, expert_weight, group_choice, local_choice, w_gate, w_up, w_down
):
    token_count, feature_count = tokens.shape
    pick_count = expert_weight.shape[1]
    group_count = lax.axis_size("g")
    lane_count = lax.axis_size("tp")
    expert_count = group_count * EPG
    capacity = pick_count * (3 * token_count // (2 * expert_count))
    group_cap = -(-(EPG * capacity // pick_count) // 16) * 16
    row_count = group_count * group_cap
    piece = feature_count // lane_count
    order = jnp.arange(token_count, dtype=jnp.int32)
    same = (group_choice[:, None] == group_choice[None, :]) & (order[:, None] > order[None, :])
    dest = group_choice * group_cap + jnp.sum(same.astype(jnp.int32), axis=1)
    pick = (jnp.arange(row_count, dtype=jnp.int32)[:, None] == dest[None, :]).astype(jnp.bfloat16)
    gate = (group_weight[:, None] * expert_weight).astype(jnp.bfloat16)
    named = local_choice[:, :, None] == jnp.arange(LANES, dtype=jnp.int32)
    gate_cols = jnp.sum(jnp.where(named, gate[:, :, None], 0), axis=1).astype(jnp.bfloat16)
    lane = lax.axis_index("tp")
    token_cols = lax.dynamic_slice_in_dim(tokens, lane * piece, piece, 1)
    cot_cols = lax.dynamic_slice_in_dim(cotangent, lane * piece, piece, 1)
    payload = jnp.concatenate([token_cols, cot_cols, gate_cols], axis=1)
    rows = jnp.dot(pick, payload, preferred_element_type=jnp.float32).astype(jnp.bfloat16)
    rows = lax.all_to_all(rows, "g", split_axis=0, concat_axis=0, tiled=True)
    rows = lax.all_gather(rows, ("e", "tp"), axis=0, tiled=False)
    rows = rows.reshape(EPG, lane_count, row_count, 2 * piece + LANES)
    all_rows = EPG * row_count
    arrived = jnp.concatenate(
        [rows[:, y, :, :piece].reshape(all_rows, piece) for y in range(lane_count)], axis=1
    )
    cot_rows = jnp.concatenate(
        [rows[:, y, :, piece : 2 * piece].reshape(all_rows, piece) for y in range(lane_count)],
        axis=1,
    )
    own = jnp.arange(LANES, dtype=jnp.int32) == lax.axis_index("e")
    gate_block = rows[:, 0, :, 2 * piece :].reshape(all_rows, LANES).astype(jnp.float32)
    gate_float = jnp.sum(jnp.where(own, gate_block, 0.0), axis=1, keepdims=True)
    first, second, third = w_gate[0], w_up[0], w_down[0]
    contract_cols = (((1,), (1,)), ((), ()))
    contract_rows = (((0,), (0,)), ((), ()))
    pre_gate = jnp.dot(arrived, first, preferred_element_type=jnp.float32)
    pre_up = jnp.dot(arrived, second, preferred_element_type=jnp.float32)
    back = lax.dot_general(cot_rows, third, contract_cols, preferred_element_type=jnp.float32)
    sigma = jax.nn.sigmoid(pre_gate)
    swish = pre_gate * sigma
    hidden = swish * pre_up
    gate_part = jnp.sum(hidden * back, axis=1, keepdims=True)
    scaled = gate_float * back
    grad_gate = (scaled * pre_up * sigma * (1.0 + pre_gate * (1.0 - sigma))).astype(jnp.bfloat16)
    grad_up = (scaled * swish).astype(jnp.bfloat16)
    weighted = (gate_float * hidden).astype(jnp.bfloat16)
    partial_rows = lax.dot_general(
        grad_gate, first, contract_cols, preferred_element_type=jnp.float32
    ) + lax.dot_general(grad_up, second, contract_cols, preferred_element_type=jnp.float32)
    partial_rows = partial_rows.astype(jnp.bfloat16)
    gate_out = jnp.where(own, gate_part, 0.0).astype(jnp.bfloat16)
    back_rows = jnp.stack(
        [
            jnp.concatenate([partial_rows[:, y * piece : (y + 1) * piece], gate_out], axis=1)
            for y in range(lane_count)
        ]
    )
    back_rows = back_rows.reshape(lane_count, EPG, row_count, piece + LANES).swapaxes(0, 1)
    back_rows = back_rows.reshape(EPG * lane_count, row_count, piece + LANES)
    returned = lax.psum_scatter(back_rows, ("e", "tp"), scatter_dimension=0, tiled=False)
    returned = lax.all_to_all(returned, "g", split_axis=0, concat_axis=0, tiled=True)
    first_grad = lax.dot_general(
        arrived, grad_gate, contract_rows, preferred_element_type=jnp.float32
    )
    second_grad = lax.dot_general(
        arrived, grad_up, contract_rows, preferred_element_type=jnp.float32
    )
    third_grad = lax.dot_general(
        weighted, cot_rows, contract_rows, preferred_element_type=jnp.float32
    )
    result = lax.dot_general(pick, returned, contract_rows, preferred_element_type=jnp.float32)
    token_grad = result[:, :piece]
    gate_grad = jnp.sum(jnp.where(named, result[:, None, piece:], 0.0), axis=2)
    gate_grad = gate_grad.astype(jnp.bfloat16).astype(jnp.float32)
    group_grad = jnp.sum(expert_weight * gate_grad, axis=1)
    expert_grad = group_weight[:, None] * gate_grad
    return (
        token_grad,
        group_grad,
        expert_grad,
        first_grad[None],
        second_grad[None],
        third_grad[None],
    )


def solution(mesh):
    lanes = mesh.shape["tp"]
    split = Mesh(mesh.devices.reshape(-1, EPG, lanes), ("g", "e", "tp"))
    ep = ("g", "e")
    in_specs = (
        P(ep, None),
        P(ep, None),
        P(ep),
        P(ep, None),
        P(ep),
        P(ep, None),
        P(ep, None, "tp"),
        P(ep, None, "tp"),
        P(ep, "tp", None),
    )
    out_specs = (
        P(ep, "tp"),
        P(ep),
        P(ep, None),
        P(ep, None, "tp"),
        P(ep, None, "tp"),
        P(ep, "tp", None),
    )
    return jax.shard_map(
        shards, mesh=split, in_specs=in_specs, out_specs=out_specs, check_vma=False
    )
```

time: 193 us -> 180 us (0.933)
  waiting for transfers between devices: 23.2 us -> 95.9 us
  blocking collectives: 97.9 us -> 27.4 us
  starting transfers between devices: 14.7 us -> 4.68 us
  local copies, waits for them, and re-layouts: 18.8 us -> 9.05 us
  matrix products: 15.6 us -> 20.3 us
    reduce_scatter x0 -> x1, waiting for transfers between devices: none -> 43.9 us  [shards(): lax.psum_scatter(back_rows, ('e', 'tp'), scatter_dimension=0, tiled=False)]
    psum x1 -> x0, blocking collectives: 36.3 us -> none  [shards(): gate_total = lax.psum(gate_part, 'tp').astype(jnp.bfloat16)]
    all_to_all x3 -> x1, blocking collectives: 61.5 us -> 27.4 us  [shards(): rows = lax.all_to_all(rows, 'g', split_axis=0, concat_axis=0, tiled=True)]
    all_gather x2 -> x1, waiting for transfers between devices: 14 us -> 46.2 us  [shards(): rows = lax.all_gather(rows, ('e', 'tp'), axis=0, tiled=False)]
    all_to_all x3 -> x1, starting transfers between devices: 14.6 us -> 4.6 us  [shards(): lax.all_to_all(returned, 'g', split_axis=0, concat_axis=0, tiled=True)]
    gather x6 -> x0, local copies, waits for them, and re-layouts: 7.6 us -> none  [the longest x2 2.09 us: shards(): jnp.take(gate_back, slot_index, axis=0).astype(jnp.float32)]
    slice x0 -> x4, local copies, waits for them, and re-layouts: none -> 6.57 us  [the longest x1 5.39 us: shards(): rows[:, y, :, :piece].reshape(all_rows, piece)]
    dot_general x5 -> x6, matrix products: 6.59 us -> 11.4 us  [the longest x1 4.39 us: shards(): lax.dot_general(arrived, grad_gate, contract_rows, preferred_element_type...]
  transfers between devices with their start and end apart: 5 -> 3, of which waited for: 3 -> 3; matrix products, arithmetic and copies ran while one was open for 12% -> 6% of each run, Pallas kernels for 0% -> 0%
where the time goes in v1:
time: 180 us
  waiting for transfers between devices  95.9 us (53%)
  blocking collectives  27.4 us (15%)
  matrix products  20.3 us (11%)
  between operations  14.3 us (8%)
  local copies, waits for them, and re-layouts  9.05 us (5%)
  other arithmetic  8.05 us (4%)
  starting transfers between devices  4.68 us (3%)
    all_gather x1, waiting for transfers between devices, shards(): rows = lax.all_gather(rows, ('e', 'tp'), axis=0, tiled=False)  46.2 us
    reduce_scatter x1, waiting for transfers between devices, shards(): lax.psum_scatter(back_rows, ('e', 'tp'), scatter_dimension=0, tiled=False)  43.9 us
    all_to_all x1, blocking collectives, shards(): rows = lax.all_to_all(rows, 'g', split_axis=0, concat_axis=0, tiled=True)  27.4 us
    all_to_all x1, waiting for transfers between devices, shards(): lax.all_to_all(returned, 'g', split_axis=0, concat_axis=0, tiled=True)  5.75 us
    slice x1, local copies, waits for them, and re-layouts, shards(): rows[:, y, :, :piece].reshape(all_rows, piece)  5.39 us
    all_to_all x1, starting transfers between devices, shards(): lax.all_to_all(returned, 'g', split_axis=0, concat_axis=0, tiled=True)  4.6 us
    dot_general x1, matrix products, shards(): lax.dot_general(arrived, grad_gate, contract_rows, preferred_element_type...  4.39 us
    dot_general x1, matrix products, shards(): lax.dot_general(arrived, grad_up, contract_rows, preferred_element_type=j...  4.24 us
  transfers between devices with their start and end apart: 3, of which 3 were waited for; matrix products, arithmetic and copies ran while one was open for 6% of the time, Pallas kernels for 0%

profile of v1, /device:TPU:0, one launch (start us, length us, event | category | flops | bytes accessed | tf_op | source)
XLA Modules:
  0.0 179.7 jit_solution(1574204471436948503)
XLA Ops:
  7.2 0.0 copy-start
  7.2 0.0 all-gather.2.cloned.1.call-start
  7.2 0.9 convert_reduce_fusion
  8.2 0.7 multiply_add_fusion
  8.8 0.7 multiply_convert_fusion.4
  9.5 0.8 fusion.19
  10.3 1.1 constant_dynamic-slice_fusion
  11.4 0.4 convolution_convert_fusion
  11.8 27.4 %all_to_all.21 = bf16[4,48,2176]{2,1,0:T(8,128)(2,1)} all-to-all(bf16[4,48,2176]{2,1,0:T(8,128)(2,1)S(1)} %bitcast.63), channel_id=1, replica_groups=mesh['g'=4,'e'=4,'tp'=2] {'g'}, dimensions={0} | all-to-all | bytes 1671168 | tf_op jit(solution)/shard_map/all_to_all | solution.py:34
  39.2 0.0 all-gather.2.cloned.1.call-update
  39.2 0.0 reduce-scatter.2.cloned.1.call-start
  39.3 46.2 %all-gather.2.cloned.1.call-done = bf16[8,192,2176]{2,1,0:T(8,128)(2,1)} async-done(((bf16[1,192,2176]{2,1,0:T(8,128)(2,1)}), bf16[8,192,2176]{2,1,0:T(8,128)(2,1)}) %all-gather.2.cloned.1.call-update) | async-done | bytes 6684688 | tf_op jit(solution)/shard_map/all_gather | solution.py:35
  85.5 5.4 %fusion.28 = (bf16[4,1,192,1024]{3,2,1,0:T(8,128)(2,1)}, bf16[4,1,192,1024]{3,2,1,0:T(8,128)(2,1)}, bf16[4,1,192,1024]{3,2,1,0:T(8,128)(2,1)S(1)}, bf16[4,1,192,1024]{3,2,1,0:T(8,128)(2,1)}) fusion(bf16[4,2,192,2176]{3,2,1,0:T(8,128)(2,1)} %bitcast.47), kind=kLoop, calls=%fused_computation.56 | loop fusion | bytes 12582912 | tf_op jit(solution)/shard_map/slice | solution.py:39
  90.9 1.1 select_reduce_fusion
  92.0 0.1 mul.72
  92.1 3.3 %fusion.6 = f32[768,256]{0,1:T(8,128)S(1)} fusion(bf16[1,2048,256]{2,1,0:T(8,128)(2,1)} %param.16, bf16[768,1024]{1,0:T(8,128)(2,1)} %bitcast.59, bf16[768,1024]{1,0:T(8,128)(2,1)} %bitcast.55), kind=kOutput, calls=%fused_computation.16 | convolution fusion | flops 811597824 | bytes 4980736 | tf_op jit(solution)/shard_map/dot_general | solution.py:52
  95.4 0.0 copy-start.10
  95.5 0.0 copy-done.1
  95.5 0.0 copy-done.9
  95.5 0.0 copy-start.3
  95.5 0.0 copy-start.4
  95.5 1.0 fusion
  96.5 0.0 copy-done.10
  96.5 0.0 copy-done
  96.5 0.6 copy-done.3
  97.2 0.5 copy-done.4
  97.6 2.2 %multiply_convert_fusion.2 = (bf16[768,256]{0,1:T(8,128)(2,1)S(1)}, bf16[768]{0:T(1024)(128)(2,1)S(1)}, bf16[768,256]{0,1:T(8,128)(2,1)S(1)}, f32[768,256]{0,1:T(8,128)}) fusion(f32[768,256]{0,1:T(8,128)S(1)} %fusion.6, f32[768,256]{0,1:T(8,128)S(1)} %fusion, f32[768]{0:T(1024)S(1)} %mul.72, bf16[1,2048,256]{2,1,0:T(8,128)(2,1)S(1)} %copy-done, ...), kind=kOutput, calls=%fused_computation.22 | convolution fusion | flops 814939392 | bytes 7344640 | tf_op jit(solution)/shard_map/dot_general | solution.py:51
  99.8 1.0 fusion.1
  100.9 0.2 copy-done.5
  101.0 1.1 add_convert_fusion
  102.1 0.3 fusion.29
  102.5 0.2 select_convert_fusion
  102.6 0.4 pad_maximum_fusion.4
  103.0 2.1 %pad_maximum_fusion = bf16[2,4,192,1152]{3,2,0,1:T(8,128)(2,1)} fusion(bf16[1,4,192,1152]{3,2,0,1:T(8,128)(2,1)S(1)} %bitcast.46, bf16[1,4,192,1152]{3,2,0,1:T(8,128)(2,1)S(1)} %bitcast.45), kind=kLoop, calls=%fused_computation.2 | loop fusion | flops 1769472 | bytes 7077888 | tf_op jit(solution)/shard_map/stack | solution.py:67
  105.1 0.0 reduce-scatter.2.cloned.1.call-update
  105.1 4.2 %convolution_bitcast_fusion.1 = f32[1,2048,256]{2,1,0:T(8,128)} fusion(bf16[768,256]{0,1:T(8,128)(2,1)S(1)} %get-tuple-element.14, bf16[768,1024]{1,0:T(8,128)(2,1)} %bitcast.60, bf16[768,1024]{1,0:T(8,128)(2,1)} %bitcast.56), kind=kOutput, calls=%fused_computation.6 | convolution fusion | flops 811597824 | bytes 5636096 | tf_op jit(solution)/shard_map/dot_general | solution.py:80
  109.4 43.9 %reduce-scatter.2.cloned.1.call-done = bf16[1,192,1152]{2,1,0:T(8,128)(2,1)} async-done(((bf16[8,192,1152]{2,1,0:T(8,128)(2,1)}), bf16[1,192,1152]{2,1,0:T(8,128)(2,1)}) %reduce-scatter.2.cloned.1.call-update) | async-done | bytes 442384 | tf_op jit(solution)/shard_map/reduce_scatter | solution.py:75
  153.2 4.6 %all-to-all-start.1 = ((bf16[4,48,1152]{2,1,0:T(8,128)(2,1)}), bf16[4,48,1152]{2,1,0:T(8,128)(2,1)S(1)}, u32[]{:S(2)}, u32[]{:S(2)}) async-start(bf16[4,48,1152]{2,1,0:T(8,128)(2,1)} %bitcast.64), calls=%async_computation.2 | async-start | bytes 884736 | tf_op jit(solution)/shard_map/all_to_all | solution.py:76
  157.8 4.4 %convolution_bitcast_fusion.2 = f32[1,2048,256]{2,1,0:T(8,128)} fusion(bf16[768,256]{0,1:T(8,128)(2,1)S(1)} %get-tuple-element.12, bf16[768,1024]{1,0:T(8,128)(2,1)} %bitcast.61, bf16[768,1024]{1,0:T(8,128)(2,1)} %bitcast.57), kind=kOutput, calls=%fused_computation.7 | convolution fusion | flops 811597824 | bytes 5636096 | tf_op jit(solution)/shard_map/dot_general | solution.py:77
  162.2 0.0 copy-start.6
  162.3 0.0 copy-start.7
  162.3 0.0 copy-start.8
  162.3 2.4 %convolution_bitcast_fusion = f32[1,256,2048]{2,1,0:T(8,128)} fusion(bf16[768,1024]{1,0:T(8,128)(2,1)S(1)} %bitcast.52, bf16[768,1024]{1,0:T(8,128)(2,1)S(1)} %bitcast.54, f32[768]{0:T(1024)S(1)} %mul.72, f32[768,256]{0,1:T(8,128)S(1)} %copy-done.11, f32[768,256]{0,1:T(8,128)S(1)} %copy-done.12), kind=kOutput, calls=%fused_computation.5 | convolution fusion | flops 812974080 | bytes 6818816 | tf_op jit(solution)/shard_map/dot_general | solution.py:83
  164.6 5.8 %all-to-all-done.1 = bf16[4,48,1152]{2,1,0:T(8,128)(2,1)S(1)} async-done(((bf16[4,48,1152]{2,1,0:T(8,128)(2,1)}), bf16[4,48,1152]{2,1,0:T(8,128)(2,1)S(1)}, u32[]{:S(2)}, u32[]{:S(2)}) %all-to-all-start.1) | async-done | bytes 442400 | tf_op jit(solution)/shard_map/all_to_all | solution.py:76
  170.4 0.3 fusion.18
  170.7 0.9 slice.43
  171.5 0.2 select_reduce_fusion.1
  171.7 1.1 convert_multiply_fusion
  (14 shorter events, 0.0 us)
Async XLA Ops:
  7.2 89.4 %copy-start = (bf16[1,2048,256]{2,1,0:T(8,128)(2,1)S(1)}, bf16[1,2048,256]{2,1,0:T(8,128)(2,1)}, u32[]{:S(2)}) copy-start(bf16[1,2048,256]{2,1,0:T(8,128)(2,1)} %param.15) | copy-start | bytes 3145732
  7.2 78.3 %all-gather.2.cloned.1.call-start = ((), (), s32[]{:S(2)}) async-start(), calls=%async_computation.3 | async-start | bytes 7520256 | tf_op jit(solution)/shard_map/all_gather | solution.py:35
  39.2 114.0 %reduce-scatter.2.cloned.1.call-start = ((), (), s32[]{:S(2)}) async-start(), calls=%async_computation.4 | async-start | bytes 3981312 | tf_op jit(solution)/shard_map/reduce_scatter | solution.py:75
  92.1 3.4 %copy-start.1 = (bf16[4,1,192,1024]{3,2,1,0:T(8,128)(2,1)S(1)}, bf16[4,1,192,1024]{3,2,1,0:T(8,128)(2,1)}, u32[]{:S(2)}) copy-start(bf16[4,1,192,1024]{3,2,1,0:T(8,128)(2,1)} %get-tuple-element.9) | copy-start | bytes 4718596
  92.1 3.4 %copy-start.9 = (bf16[1,256,2048]{2,1,0:T(8,128)(2,1)S(1)}, bf16[1,256,2048]{2,1,0:T(8,128)(2,1)}, u32[]{:S(2)}) copy-start(bf16[1,256,2048]{2,1,0:T(8,128)(2,1)} %param.17) | copy-start | bytes 3145732
  95.4 1.1 copy-start.10
  95.5 1.7 copy-start.3
  95.5 2.1 %copy-start.4 = (bf16[4,1,192,1024]{3,2,1,0:T(8,128)(2,1)S(1)}, bf16[4,1,192,1024]{3,2,1,0:T(8,128)(2,1)}, u32[]{:S(2)}) copy-start(bf16[4,1,192,1024]{3,2,1,0:T(8,128)(2,1)} %get-tuple-element.7) | copy-start | bytes 4718596
  99.8 1.2 copy-start.5
  153.2 17.2 %all-to-all-start.1 = ((bf16[4,48,1152]{2,1,0:T(8,128)(2,1)}), bf16[4,48,1152]{2,1,0:T(8,128)(2,1)S(1)}, u32[]{:S(2)}, u32[]{:S(2)}) async-start(bf16[4,48,1152]{2,1,0:T(8,128)(2,1)} %bitcast.64), calls=%async_computation.2 | async-start | bytes 884736 | tf_op jit(solution)/shard_map/all_to_all | solution.py:76
  157.8 4.4 %copy-start.2 = (bf16[4,1,192,1024]{3,2,1,0:T(8,128)(2,1)S(1)}, bf16[4,1,192,1024]{3,2,1,0:T(8,128)(2,1)}, u32[]{:S(2)}) copy-start(bf16[4,1,192,1024]{3,2,1,0:T(8,128)(2,1)} %get-tuple-element.9) | copy-start | bytes 4718596
  157.8 4.4 %copy-start.11 = (f32[768,256]{0,1:T(8,128)S(1)}, f32[768,256]{0,1:T(8,128)}, u32[]{:S(2)}) copy-start(f32[768,256]{0,1:T(8,128)} %copy-done.10) | copy-start | bytes 2359300
  157.8 4.4 %copy-start.12 = (f32[768,256]{0,1:T(8,128)S(1)}, f32[768,256]{0,1:T(8,128)}, u32[]{:S(2)}) copy-start(f32[768,256]{0,1:T(8,128)} %get-tuple-element.19) | copy-start | bytes 2359300
  162.2 9.3 %copy-start.6 = (s32[128,2]{0,1:T(2,128)S(1)}, s32[128,2]{0,1:T(2,128)}, u32[]{:S(2)}) copy-start(s32[128,2]{0,1:T(2,128)} %param.14) | copy-start | bytes 3076
  162.3 9.5 %copy-start.7 = (f32[128,2]{0,1:T(2,128)S(1)}, f32[128,2]{0,1:T(2,128)}, u32[]{:S(2)}) copy-start(f32[128,2]{0,1:T(2,128)} %param.12) | copy-start | bytes 3076
  162.3 9.5 %copy-start.8 = (f32[128]{0:T(128)S(1)}, f32[128]{0:T(128)}, u32[]{:S(2)}) copy-start(f32[128]{0:T(128)} %param.11) | copy-start | bytes 1540
Sparse Core Ops, SparseCore 0:
  39.3 46.1 all-gather.1
  105.2 47.9 reduce-scatter.1

commit v2 on v1

--- a/solution.py
+++ b/solution.py
@@ -1,10 +1,301 @@
+import functools
+
 import jax
 import jax.numpy as jnp
 from jax import lax
+from jax.experimental import pallas as pl
+from jax.experimental.pallas import tpu as pltpu
 from jax.sharding import Mesh, PartitionSpec as P
 
 EPG = 4
 LANES = 128
+
+MESH = pl.DeviceIdType.MESH
+
+
+def place():
+    g, e, y = lax.axis_index("g"), lax.axis_index("e"), lax.axis_index("tp")
+    x, c = e // 2, e % 2
+    return g, e, y, x, c
+
+
+def greet(devices):
+    barrier = pltpu.get_barrier_semaphore()
+    for device in devices:
+        pl.semaphore_signal(barrier, inc=1, device_id=device, device_id_type=MESH)
+    pl.semaphore_wait(barrier, len(devices))
+
+
+class Copies:
+    def __init__(self, send_sem, recv_sem):
+        self.send_sem, self.recv_sem, self.made = send_sem, recv_sem, []
+
+    def start(self, src, dst, device):
+        number = len(self.made)
+        copy = pltpu.make_async_remote_copy(
+            src_ref=src,
+            dst_ref=dst,
+            send_sem=self.send_sem.at[number],
+            recv_sem=self.recv_sem.at[number],
+            device_id=device,
+            device_id_type=MESH,
+        )
+        copy.start()
+        self.made.append(copy)
+        return copy
+
+    def finish(self):
+        for copy in self.made:
+            copy.wait_send()
+
+
+def window(start, size, unit):
+    return pl.ds(pl.multiple_of(start, unit), size)
+
+
+def forward_count(groups, lanes):
+    return (groups - 1) * 3 + groups * (3 * (lanes - 1) + 9)
+
+
+def forward_kernel(groups, lanes, cap, piece, tok_in, cot_in, gate_in, tok, cot, gate, send, recv, loc):
+    g, e, y, x, c = place()
+    rows = groups * cap
+    ex, ec, exc = (1 - x) * 2 + c, x * 2 + (1 - c), (1 - x) * 2 + (1 - c)
+    others = [(g, e, lax.rem(y + r, lanes)) for r in range(1, lanes)]
+    greet(
+        [(lax.rem(g + d, groups), e, y) for d in range(1, groups)]
+        + others
+        + [(g, ex, y), (g, ec, y), (g, exc, y)]
+    )
+    copies = Copies(send, recv)
+    cols = window(y * piece, piece, LANES)
+
+    def block(ref, owner, source, columns=slice(None)):
+        return ref.at[window(owner * rows + source * cap, cap, 16), columns]
+
+    def inner(ref, group):
+        return ref.at[window(group * cap, cap, 16), :]
+
+    first = []
+    pairs = ((tok_in, tok, cols), (cot_in, cot, cols), (gate_in, gate, slice(None)))
+    for d in range(groups):
+        target = lax.rem(g - d + groups, groups)
+        made = []
+        for i, (src, dst, columns) in enumerate(pairs):
+            if d == 0:
+                copy = pltpu.make_async_copy(inner(src, g), block(dst, e, g, columns), loc.at[i])
+                copy.start()
+            else:
+                copy = copies.start(inner(src, target), block(dst, e, g, columns), (target, e, y))
+            made.append(copy)
+        first.append(made)
+    state = [dict() for _ in range(groups)]
+    last = []
+
+    def stage_a(d):
+        source = lax.rem(g + d, groups)
+        for copy in first[d]:
+            if d == 0:
+                copy.wait()
+            else:
+                copy.wait_recv()
+        own_t, own_c = block(tok, e, source, cols), block(cot, e, source, cols)
+        state[d]["tl"] = [copies.start(own_t, own_t, device) for device in others]
+        state[d]["cx"] = copies.start(own_c, own_c, (g, ex, y))
+        state[d]["cl"] = [copies.start(own_c, own_c, device) for device in others]
+        own_g = block(gate, e, source)
+        for peer in (ex, ec, exc):
+            last.append(copies.start(own_g, own_g, (g, peer, y)))
+
+    def stage_b(d):
+        source = lax.rem(g + d, groups)
+        for copy in state[d]["tl"]:
+            copy.wait_recv()
+        full = block(tok, e, source)
+        state[d]["tx"] = copies.start(full, full, (g, ex, y))
+        state[d]["cx"].wait_recv()
+        part = block(cot, ex, source, cols)
+        state[d]["cxl"] = [copies.start(part, part, device) for device in others]
+        last.append(copies.start(full, full, (g, ec, y)))
+
+    def stage_c(d):
+        source = lax.rem(g + d, groups)
+        for copy in state[d]["cl"]:
+            copy.wait_recv()
+        full = block(cot, e, source)
+        last.append(copies.start(full, full, (g, ec, y)))
+        state[d]["tx"].wait_recv()
+        full = block(tok, ex, source)
+        last.append(copies.start(full, full, (g, ec, y)))
+        for copy in state[d]["cxl"]:
+            copy.wait_recv()
+        full = block(cot, ex, source)
+        last.append(copies.start(full, full, (g, ec, y)))
+
+    for step in range(groups + 2):
+        if step < groups:
+            stage_a(step)
+        if 0 <= step - 1 < groups:
+            stage_b(step - 1)
+        if 0 <= step - 2 < groups:
+            stage_c(step - 2)
+    for copy in last:
+        copy.wait_recv()
+    copies.finish()
+
+
+def forward(tok_in, cot_in, gate_in, groups, lanes, cap, piece):
+    all_rows = EPG * groups * cap
+    count = forward_count(groups, lanes)
+    vmem = pl.BlockSpec(memory_space=pltpu.VMEM)
+    return pl.pallas_call(
+        functools.partial(forward_kernel, groups, lanes, cap, piece),
+        out_shape=(
+            jax.ShapeDtypeStruct((all_rows, lanes * piece), jnp.bfloat16),
+            jax.ShapeDtypeStruct((all_rows, lanes * piece), jnp.bfloat16),
+            jax.ShapeDtypeStruct((all_rows, LANES), jnp.bfloat16),
+        ),
+        in_specs=[vmem] * 3,
+        out_specs=(vmem,) * 3,
+        scratch_shapes=[
+            pltpu.SemaphoreType.DMA((count,)),
+            pltpu.SemaphoreType.DMA((count,)),
+            pltpu.SemaphoreType.DMA((3,)),
+        ],
+        compiler_params=pltpu.CompilerParams(collective_id=0, has_side_effects=True),
+        name="forward_exchange",
+    )(tok_in, cot_in, gate_in)
+
+
+def add(*parts):
+    total = parts[0].astype(jnp.float32)
+    for part in parts[1:]:
+        total = total + part.astype(jnp.float32)
+    return total.astype(jnp.bfloat16)
+
+
+def return_kernel(
+    groups, lanes, cap, wide0, wide1, part, out, rc, s1, rx0, s2a, rl0, rl1, s2b, rx1, done, send, recv
+):
+    g, e, y, x, c = place()
+    rows = groups * cap
+    ex, ec = (1 - x) * 2 + c, x * 2 + (1 - c)
+    others = [(g, e, lax.rem(y + r, lanes)) for r in range(1, lanes)]
+    greet(
+        [(lax.rem(g + d, groups), e, y) for d in range(1, groups)]
+        + others
+        + [(g, ex, y), (g, ec, y)]
+    )
+    copies = Copies(send, recv)
+    all0 = lanes * wide0
+    head, tail = pl.ds(0, all0), pl.ds(all0, lanes * wide1)
+
+    def at(index, source):
+        return window(index * rows + source * cap, cap, 16)
+
+    def lane0(lane):
+        return window(lane * wide0, wide0, LANES)
+
+    def lane1(lane):
+        return window(all0 + lane * wide1, wide1, LANES)
+
+    order = list(range(1, groups)) + [0]
+    sources = [lax.rem(g + d, groups) for d in order]
+    state = [dict() for _ in order]
+    for i, s in enumerate(sources):
+        state[i]["core"] = [
+            copies.start(part.at[at(2 * k + 1 - c, s), :], rc.at[at(k, s), :], (g, ec, y))
+            for k in range(2)
+        ]
+
+    def stage_a(i):
+        s = sources[i]
+        for k in range(2):
+            state[i]["core"][k].wait_recv()
+            for columns in (head, tail):
+                s1[at(k, s), columns] = add(part[at(2 * k + c, s), columns], rc[at(k, s), columns])
+        state[i]["x0"] = copies.start(s1.at[at(1 - x, s), head], rx0.at[at(0, s), :], (g, ex, y))
+        state[i]["l1"] = [
+            copies.start(
+                s1.at[at(k, s), lane1(device[2])], rl1.at[at(2 * r + k, s), :], device
+            )
+            for r, device in enumerate(others)
+            for k in range(2)
+        ]
+
+    def stage_b(i):
+        s = sources[i]
+        state[i]["x0"].wait_recv()
+        s2a[at(0, s), :] = add(s1[at(x, s), head], rx0[at(0, s), :])
+        state[i]["l0"] = [
+            copies.start(s2a.at[at(0, s), lane0(device[2])], rl0.at[at(r, s), :], device)
+            for r, device in enumerate(others)
+        ]
+        for copy in state[i]["l1"]:
+            copy.wait_recv()
+        for k in range(2):
+            s2b[at(k, s), :] = add(
+                s1[at(k, s), lane1(y)], *[rl1[at(2 * r + k, s), :] for r in range(lanes - 1)]
+            )
+        state[i]["x1"] = copies.start(s2b.at[at(1 - x, s), :], rx1.at[at(0, s), :], (g, ex, y))
+
+    def stage_c(i):
+        s = sources[i]
+        target = out if order[i] == 0 else done
+        for copy in state[i]["l0"]:
+            copy.wait_recv()
+        target[at(0, s), pl.ds(0, wide0)] = add(
+            s2a[at(0, s), lane0(y)], *[rl0[at(r, s), :] for r in range(lanes - 1)]
+        )
+        state[i]["x1"].wait_recv()
+        target[at(0, s), pl.ds(wide0, wide1)] = add(s2b[at(x, s), :], rx1[at(0, s), :])
+        if order[i] != 0:
+            state[i]["z"] = copies.start(done.at[at(0, s), :], out.at[at(0, g), :], (s, e, y))
+
+    for step in range(groups + 2):
+        if step < groups:
+            stage_a(step)
+        if 0 <= step - 1 < groups:
+            stage_b(step - 1)
+        if 0 <= step - 2 < groups:
+            stage_c(step - 2)
+    for i in range(groups):
+        if order[i] != 0:
+            state[i]["z"].wait_recv()
+    copies.finish()
+
+
+def give_back(part, groups, lanes, cap, wide0, wide1):
+    rows = groups * cap
+    count = (groups - 1) + groups * (4 + 3 * (lanes - 1))
+    vmem = pl.BlockSpec(memory_space=pltpu.VMEM)
+    wide = lanes * (wide0 + wide1)
+    far = max(lanes - 1, 1)
+
+    def buffer(height, width):
+        return pltpu.VMEM((height, width), jnp.bfloat16)
+
+    return pl.pallas_call(
+        functools.partial(return_kernel, groups, lanes, cap, wide0, wide1),
+        out_shape=jax.ShapeDtypeStruct((rows, wide0 + wide1), jnp.bfloat16),
+        in_specs=[vmem],
+        out_specs=vmem,
+        scratch_shapes=[
+            buffer(2 * rows, wide),
+            buffer(2 * rows, wide),
+            buffer(rows, lanes * wide0),
+            buffer(rows, lanes * wide0),
+            buffer(far * rows, wide0),
+            buffer(far * 2 * rows, wide1),
+            buffer(2 * rows, wide1),
+            buffer(rows, wide1),
+            buffer(rows, wide0 + wide1),
+            pltpu.SemaphoreType.DMA((count,)),
+            pltpu.SemaphoreType.DMA((count,)),
+        ],
+        compiler_params=pltpu.CompilerParams(collective_id=1, has_side_effects=True),
+        name="return_exchange",
+    )(part)
 
 
 def shards(
@@ -31,19 +322,17 @@
     cot_cols = lax.dynamic_slice_in_dim(cotangent, lane * piece, piece, 1)
     payload = jnp.concatenate([token_cols, cot_cols, gate_cols], axis=1)
     rows = jnp.dot(pick, payload, preferred_element_type=jnp.float32).astype(jnp.bfloat16)
-    rows = lax.all_to_all(rows, "g", split_axis=0, concat_axis=0, tiled=True)
-    rows = lax.all_gather(rows, ("e", "tp"), axis=0, tiled=False)
-    rows = rows.reshape(EPG, lane_count, row_count, 2 * piece + LANES)
-    all_rows = EPG * row_count
-    arrived = jnp.concatenate(
-        [rows[:, y, :, :piece].reshape(all_rows, piece) for y in range(lane_count)], axis=1
-    )
-    cot_rows = jnp.concatenate(
-        [rows[:, y, :, piece : 2 * piece].reshape(all_rows, piece) for y in range(lane_count)],
-        axis=1,
+    arrived, cot_rows, gate_block = forward(
+        rows[:, :piece],
+        rows[:, piece : 2 * piece],
+        rows[:, 2 * piece :],
+        group_count,
+        lane_count,
+        group_cap,
+        piece,
     )
     own = jnp.arange(LANES, dtype=jnp.int32) == lax.axis_index("e")
-    gate_block = rows[:, 0, :, 2 * piece :].reshape(all_rows, LANES).astype(jnp.float32)
+    gate_block = gate_block.astype(jnp.float32)
     gate_float = jnp.sum(jnp.where(own, gate_block, 0.0), axis=1, keepdims=True)
     first, second, third = w_gate[0], w_up[0], w_down[0]
     contract_cols = (((1,), (1,)), ((), ()))
@@ -64,16 +353,18 @@
     ) + lax.dot_general(grad_up, second, contract_cols, preferred_element_type=jnp.float32)
     partial_rows = partial_rows.astype(jnp.bfloat16)
     gate_out = jnp.where(own, gate_part, 0.0).astype(jnp.bfloat16)
-    back_rows = jnp.stack(
-        [
-            jnp.concatenate([partial_rows[:, y * piece : (y + 1) * piece], gate_out], axis=1)
+    wide1 = (piece + LANES) // (2 * LANES) * LANES
+    wide0 = piece + LANES - wide1
+    back_rows = jnp.concatenate(
+        [partial_rows[:, y * piece : y * piece + wide0] for y in range(lane_count)]
+        + [
+            column
             for y in range(lane_count)
-        ]
-    )
-    back_rows = back_rows.reshape(lane_count, EPG, row_count, piece + LANES).swapaxes(0, 1)
-    back_rows = back_rows.reshape(EPG * lane_count, row_count, piece + LANES)
-    returned = lax.psum_scatter(back_rows, ("e", "tp"), scatter_dimension=0, tiled=False)
-    returned = lax.all_to_all(returned, "g", split_axis=0, concat_axis=0, tiled=True)
+            for column in (partial_rows[:, y * piece + wide0 : (y + 1) * piece], gate_out)
+        ],
+        axis=1,
+    )
+    returned = give_back(back_rows, group_count, lane_count, group_cap, wide0, wide1)
     first_grad = lax.dot_general(
         arrived, grad_gate, contract_rows, preferred_element_type=jnp.float32
     )

time: 180 us -> 111 us (0.62)
  waiting for transfers between devices: 95.9 us -> 0 us
  Pallas kernels: 0 us -> 77.3 us
  blocking collectives: 27.4 us -> 0 us
  between operations: 14.3 us -> 0.81 us
  starting transfers between devices: 4.68 us -> 0 us
  matrix products: 20.3 us -> 16.4 us
    pallas_call x0 -> x2, Pallas kernels: none -> 77.3 us  [the longest x1 49.5 us: forward(): pl.pallas_call(functools.partial(forward_kernel, groups, lanes, cap, piec...]
    all_gather x1 -> x0, waiting for transfers between devices: 46.2 us -> none  [shards(): rows = lax.all_gather(rows, ('e', 'tp'), axis=0, tiled=False)]
    reduce_scatter x1 -> x0, waiting for transfers between devices: 43.9 us -> none  [shards(): lax.psum_scatter(back_rows, ('e', 'tp'), scatter_dimension=0, tiled=False)]
    all_to_all x1 -> x0, blocking collectives: 27.4 us -> none  [shards(): rows = lax.all_to_all(rows, 'g', split_axis=0, concat_axis=0, tiled=True)]
    all_to_all x1 -> x0, waiting for transfers between devices: 5.75 us -> none  [shards(): lax.all_to_all(returned, 'g', split_axis=0, concat_axis=0, tiled=True)]
    all_to_all x1 -> x0, starting transfers between devices: 4.6 us -> none  [shards(): lax.all_to_all(returned, 'g', split_axis=0, concat_axis=0, tiled=True)]
    slice x2, local copies, waits for them, and re-layouts: 5.72 us -> 1.6 us  [the longest x1 0.98 us: shards(): rows[:, piece:2 * piece]]
    unnamed x26 -> x20, local copies, waits for them, and re-layouts: 1.32 us -> 5.17 us
  transfers between devices with their start and end apart: 3 -> 0, of which waited for: 3 -> 0; matrix products, arithmetic and copies ran while one was open for 6% -> 0% of each run, Pallas kernels for 0% -> 0%
where the time goes in v2:
time: 111 us
  Pallas kernels  77.3 us (70%)
  matrix products  16.4 us (15%)
  local copies, waits for them, and re-layouts  8.69 us (8%)
  other arithmetic  7.36 us (7%)
    pallas_call x1, Pallas kernels, forward(): pl.pallas_call(functools.partial(forward_kernel, groups, lanes, cap, piec...  49.5 us
    pallas_call x1, Pallas kernels, give_back(): pl.pallas_call(functools.partial(return_kernel, groups, lanes, cap, wide0...  27.8 us
    unnamed x20, local copies, waits for them, and re-layouts  5.17 us
    dot_general x1, matrix products, shards(): pre_gate = jnp.dot(arrived, first, preferred_element_type=jnp.float32)  2.9 us
    dot_general x1, matrix products, shards(): lax.dot_general(arrived, grad_up, contract_rows, preferred_element_type=j...  2.41 us
    dot_general x1, matrix products, shards(): lax.dot_general(arrived, grad_gate, contract_rows, preferred_element_type...  2.4 us
    dot_general x1, matrix products, shards(): lax.dot_general(weighted, cot_rows, contract_rows, preferred_element_type...  2.36 us

profile of v2, /device:TPU:0, one launch (start us, length us, event | category | flops | bytes accessed | tf_op | source)
XLA Modules:
  0.0 110.5 jit_solution(17916120858615688190)
XLA Ops:
  0.6 0.0 copy-start
  0.7 0.8 multiply_convert_fusion.4
  1.4 0.9 convert_reduce_fusion
  2.3 0.7 multiply_add_fusion
  3.0 0.8 fusion.21
  3.8 1.1 constant_dynamic-slice_fusion
  4.9 0.4 convolution_convert_fusion
  5.3 0.6 slice.38.gate_in
  5.9 1.0 fusion.28
  6.9 0.0 copy-start.2
  6.9 49.5 %forward_exchange.1 = (bf16[768,2048]{1,0:T(8,128)(2,1)}, bf16[768,2048]{1,0:T(8,128)(2,1)}, bf16[768,128]{1,0:T(8,128)(2,1)}) custom-call(bf16[192,1024]{1,0:T(8,128)(2,1)} %get-tuple-element.16.tok_in, bf16[192,1024]{1,0:T(8,128)(2,1)} %get-tuple-element.15.cot_in, bf16[192,128]{1,0:T(8,128)(2,1)} %slice.38.gate_in), custom_call_target="tpu_custom_call" | custom-call | tf_op jit(solution)/shard_map/forward_exchange/pallas_call | solution.py:151
  56.4 0.0 copy-start.1
  56.4 1.2 %select_reduce_fusion = f32[768]{0:T(1024)S(1)} fusion(bf16[768,128]{1,0:T(8,128)(2,1)} %get-tuple-element.9, pred[128]{0:T(512)(128)(4,1)S(1)} %iota_compare_fusion.5), kind=kLoop, calls=%fused_computation.31 | loop fusion | flops 294144 | bytes 199808 | tf_op jit(solution)/shard_map/reduce_sum | solution.py:336
  57.6 0.0 copy-done
  57.6 2.9 %fusion.2 = f32[768,256]{0,1:T(8,128)S(1)} fusion(bf16[768,2048]{1,0:T(8,128)(2,1)} %get-tuple-element.11, bf16[1,2048,256]{2,1,0:T(8,128)(2,1)S(1)} %copy-done), kind=kOutput, calls=%fused_computation.7 | convolution fusion | flops 805306368 | bytes 4980736 | tf_op jit(solution)/shard_map/dot_general | solution.py:340
  60.5 0.0 copy-done.2
  60.5 0.0 copy-done.1
  60.5 0.0 copy-start.6
  60.5 0.0 copy-start.7
  60.6 1.1 %fusion.5 = f32[768,256]{0,1:T(8,128)S(1)} fusion(bf16[768,2048]{1,0:T(8,128)(2,1)S(1)} %copy-done.1, bf16[1,2048,256]{2,1,0:T(8,128)(2,1)S(1)} %copy-done.2), kind=kOutput, calls=%fused_computation.10 | convolution fusion | flops 805306368 | bytes 4980736 | tf_op jit(solution)/shard_map/dot_general | solution.py:341
  61.7 0.8 copy-done.6
  62.4 0.3 copy-done.7
  62.7 1.4 %multiply_reduce_fusion = (bf16[768]{0:T(1024)(128)(2,1)S(1)}, bf16[768,256]{0,1:T(8,128)(2,1)S(1)}, bf16[768,256]{0,1:T(8,128)(2,1)S(1)}) fusion(f32[768,256]{0,1:T(8,128)S(1)} %fusion.5, f32[768,256]{0,1:T(8,128)S(1)} %fusion.2, f32[768]{0:T(1024)S(1)} %select_reduce_fusion, bf16[768,2048]{1,0:T(8,128)(2,1)S(1)} %copy-done.6, ...), kind=kOutput, calls=%fused_computation.17 | convolution fusion | flops 808647936 | bytes 6558208 | tf_op jit(solution)/shard_map/dot_general | solution.py:342
  64.1 2.4 %convolution_bitcast_fusion = f32[1,256,2048]{2,1,0:T(8,128)} fusion(bf16[768,2048]{1,0:T(8,128)(2,1)S(1)} %copy-done.6, f32[768]{0:T(1024)S(1)} %select_reduce_fusion, f32[768,256]{0,1:T(8,128)S(1)} %fusion.5, f32[768,256]{0,1:T(8,128)S(1)} %fusion.2), kind=kOutput, calls=%fused_computation.2 | convolution fusion | flops 806682624 | bytes 6818816 | tf_op jit(solution)/shard_map/dot_general | solution.py:374
  66.5 2.4 %convolution_bitcast_fusion.2 = f32[1,2048,256]{2,1,0:T(8,128)} fusion(bf16[768,2048]{1,0:T(8,128)(2,1)S(1)} %copy-done.1, bf16[768,256]{0,1:T(8,128)(2,1)S(1)} %get-tuple-element.13), kind=kOutput, calls=%fused_computation.4 | convolution fusion | flops 805306368 | bytes 5636096 | tf_op jit(solution)/shard_map/dot_general | solution.py:368
  68.9 2.4 %convolution_bitcast_fusion.1 = f32[1,2048,256]{2,1,0:T(8,128)} fusion(bf16[768,2048]{1,0:T(8,128)(2,1)S(1)} %copy-done.1, bf16[768,256]{0,1:T(8,128)(2,1)S(1)} %get-tuple-element.14), kind=kOutput, calls=%fused_computation.3 | convolution fusion | flops 805306368 | bytes 5636096 | tf_op jit(solution)/shard_map/dot_general | solution.py:371
  71.3 1.0 fusion
  72.3 1.0 add_convert_fusion
  73.4 1.1 %slice_dynamic-update-slice_fusion.1 = bf16[768,2304]{1,0:T(8,128)(2,1)} fusion(bf16[768,2048]{1,0:T(8,128)(2,1)S(1)} %add_convert_fusion), kind=kLoop, calls=%fused_computation.15 | loop fusion | bytes 1966080
  74.5 1.1 %slice_dynamic-update-slice_fusion = bf16[768,2304]{1,0:T(8,128)(2,1)} fusion(bf16[768,2304]{1,0:T(8,128)(2,1)} %slice_dynamic-update-slice_fusion.1, bf16[768,2048]{1,0:T(8,128)(2,1)S(1)} %add_convert_fusion), kind=kLoop, calls=%fused_computation.14 | loop fusion | bytes 1966080
  75.6 0.9 slice_dynamic-update-slice_fusion.3
  76.6 0.9 fusion.17
  77.4 0.9 slice_dynamic-update-slice_fusion.2
  78.4 0.9 fusion.18.part
  79.2 0.0 copy-start.3
  79.2 0.0 copy-start.4
  79.2 0.0 copy-start.5
  79.2 27.8 %return_exchange.1 = bf16[192,1152]{1,0:T(8,128)(2,1)} custom-call(bf16[768,2304]{1,0:T(8,128)(2,1)} %fusion.18.part), custom_call_target="tpu_custom_call" | custom-call | tf_op jit(solution)/shard_map/return_exchange/pallas_call | solution.py:278
  107.1 1.3 %fusion.20 = f32[128,1152]{1,0:T(8,128)S(1)} fusion(bf16[192,1152]{1,0:T(8,128)(2,1)} %return_exchange.1, s32[128]{0:T(128)S(1)} %multiply_add_fusion), kind=kOutput, calls=%fused_computation.39 | convolution fusion | flops 56647680 | bytes 1032704 | tf_op jit(solution)/shard_map/dot_general | solution.py:377
  108.4 0.8 slice.43
  109.2 0.0 copy-done.3
  109.2 0.2 select_reduce_fusion.1
  109.4 0.0 copy-done.4
  109.4 0.0 copy-done.5
  109.4 1.1 convert_multiply_fusion
  (2 shorter events, 0.0 us)
Async XLA Ops:
  0.6 57.0 %copy-start = (bf16[1,2048,256]{2,1,0:T(8,128)(2,1)S(1)}, bf16[1,2048,256]{2,1,0:T(8,128)(2,1)}, u32[]{:S(2)}) copy-start(bf16[1,2048,256]{2,1,0:T(8,128)(2,1)} %param.15) | copy-start | bytes 3145732
  6.9 53.6 %copy-start.2 = (bf16[1,2048,256]{2,1,0:T(8,128)(2,1)S(1)}, bf16[1,2048,256]{2,1,0:T(8,128)(2,1)}, u32[]{:S(2)}) copy-start(bf16[1,2048,256]{2,1,0:T(8,128)(2,1)} %param.16) | copy-start | bytes 3145732
  56.4 4.2 %copy-start.1 = (bf16[768,2048]{1,0:T(8,128)(2,1)S(1)}, bf16[768,2048]{1,0:T(8,128)(2,1)}, u32[]{:S(2)}) copy-start(bf16[768,2048]{1,0:T(8,128)(2,1)} %get-tuple-element.11) | copy-start | bytes 9437188
  60.5 1.9 %copy-start.6 = (bf16[768,2048]{1,0:T(8,128)(2,1)S(1)}, bf16[768,2048]{1,0:T(8,128)(2,1)}, u32[]{:S(2)}) copy-start(bf16[768,2048]{1,0:T(8,128)(2,1)} %get-tuple-element.10) | copy-start | bytes 9437188
  60.5 2.2 %copy-start.7 = (bf16[1,256,2048]{2,1,0:T(8,128)(2,1)S(1)}, bf16[1,256,2048]{2,1,0:T(8,128)(2,1)}, u32[]{:S(2)}) copy-start(bf16[1,256,2048]{2,1,0:T(8,128)(2,1)} %param.17) | copy-start | bytes 3145732
  79.2 30.0 %copy-start.3 = (s32[128,2]{0,1:T(2,128)S(1)}, s32[128,2]{0,1:T(2,128)}, u32[]{:S(2)}) copy-start(s32[128,2]{0,1:T(2,128)} %param.14) | copy-start | bytes 3076
  79.2 30.2 %copy-start.4 = (f32[128,2]{0,1:T(2,128)S(1)}, f32[128,2]{0,1:T(2,128)}, u32[]{:S(2)}) copy-start(f32[128,2]{0,1:T(2,128)} %param.12) | copy-start | bytes 3076
  79.2 30.2 %copy-start.5 = (f32[128]{0:T(128)S(1)}, f32[128]{0:T(128)}, u32[]{:S(2)}) copy-start(f32[128]{0:T(128)} %param.11) | copy-start | bytes 1540

commit v3 on v2

--- a/solution.py
+++ b/solution.py
@@ -17,6 +17,17 @@
     g, e, y = lax.axis_index("g"), lax.axis_index("e"), lax.axis_index("tp")
     x, c = e // 2, e % 2
     return g, e, y, x, c
+
+
+def partner(g, d, groups, sign):
+    if groups & (groups - 1):
+        return lax.rem(g + sign * d + groups, groups)
+    met, bit = g, 1
+    while bit < groups:
+        if d & bit:
+            met = met + bit - 2 * bit * ((g // bit) % 2)
+        bit *= 2
+    return met
 
 
 def greet(devices):
@@ -79,7 +90,7 @@
     first = []
     pairs = ((tok_in, tok, cols), (cot_in, cot, cols), (gate_in, gate, slice(None)))
     for d in range(groups):
-        target = lax.rem(g - d + groups, groups)
+        target = partner(g, d, groups, -1)
         made = []
         for i, (src, dst, columns) in enumerate(pairs):
             if d == 0:
@@ -93,7 +104,7 @@
     last = []
 
     def stage_a(d):
-        source = lax.rem(g + d, groups)
+        source = partner(g, d, groups, 1)
         for copy in first[d]:
             if d == 0:
                 copy.wait()
@@ -108,7 +119,7 @@
             last.append(copies.start(own_g, own_g, (g, peer, y)))
 
     def stage_b(d):
-        source = lax.rem(g + d, groups)
+        source = partner(g, d, groups, 1)
         for copy in state[d]["tl"]:
             copy.wait_recv()
         full = block(tok, e, source)
@@ -119,7 +130,7 @@
         last.append(copies.start(full, full, (g, ec, y)))
 
     def stage_c(d):
-        source = lax.rem(g + d, groups)
+        source = partner(g, d, groups, 1)
         for copy in state[d]["cl"]:
             copy.wait_recv()
         full = block(cot, e, source)
@@ -199,8 +210,8 @@
     def lane1(lane):
         return window(all0 + lane * wide1, wide1, LANES)
 
-    order = list(range(1, groups)) + [0]
-    sources = [lax.rem(g + d, groups) for d in order]
+    order = list(range(groups // 2, groups)) + list(range(1, groups // 2)) + [0]
+    sources = [partner(g, d, groups, 1) for d in order]
     state = [dict() for _ in order]
     for i, s in enumerate(sources):
         state[i]["core"] = [

time: 111 us -> 108 us (0.973)
  Pallas kernels: 77.3 us -> 74.5 us
    pallas_call x1, Pallas kernels: 27.8 us -> 26.1 us  [give_back(): pl.pallas_call(functools.partial(return_kernel, groups, lanes, cap, wide0...]
    pallas_call x1, Pallas kernels: 49.5 us -> 48.3 us  [forward(): pl.pallas_call(functools.partial(forward_kernel, groups, lanes, cap, piec...]
where the time goes in v3:
time: 108 us
  Pallas kernels  74.5 us (69%)
  matrix products  16.4 us (15%)
  local copies, waits for them, and re-layouts  8.69 us (8%)
  other arithmetic  7.36 us (7%)
    pallas_call x1, Pallas kernels, forward(): pl.pallas_call(functools.partial(forward_kernel, groups, lanes, cap, piec...  48.3 us
    pallas_call x1, Pallas kernels, give_back(): pl.pallas_call(functools.partial(return_kernel, groups, lanes, cap, wide0...  26.1 us
    unnamed x20, local copies, waits for them, and re-layouts  5.17 us
    dot_general x1, matrix products, shards(): pre_gate = jnp.dot(arrived, first, preferred_element_type=jnp.float32)  2.9 us
    dot_general x1, matrix products, shards(): lax.dot_general(arrived, grad_up, contract_rows, preferred_element_type=j...  2.41 us
    dot_general x1, matrix products, shards(): lax.dot_general(arrived, grad_gate, contract_rows, preferred_element_type...  2.4 us
    dot_general x1, matrix products, shards(): lax.dot_general(weighted, cot_rows, contract_rows, preferred_element_type...  2.37 us

profile of v3, /device:TPU:0, one launch (start us, length us, event | category | flops | bytes accessed | tf_op | source)
XLA Modules:
  0.0 107.7 jit_solution(14965847942322609312)
XLA Ops:
  0.6 0.0 copy-start
  0.7 0.8 multiply_convert_fusion.4
  1.4 0.9 convert_reduce_fusion
  2.3 0.7 multiply_add_fusion
  3.0 0.8 fusion.21
  3.8 1.1 constant_dynamic-slice_fusion
  4.9 0.4 convolution_convert_fusion
  5.3 0.6 slice.38.gate_in
  5.9 1.0 fusion.28
  6.9 0.0 copy-start.2
  6.9 48.3 %forward_exchange.1 = (bf16[768,2048]{1,0:T(8,128)(2,1)}, bf16[768,2048]{1,0:T(8,128)(2,1)}, bf16[768,128]{1,0:T(8,128)(2,1)}) custom-call(bf16[192,1024]{1,0:T(8,128)(2,1)} %get-tuple-element.16.tok_in, bf16[192,1024]{1,0:T(8,128)(2,1)} %get-tuple-element.15.cot_in, bf16[192,128]{1,0:T(8,128)(2,1)} %slice.38.gate_in), custom_call_target="tpu_custom_call" | custom-call | tf_op jit(solution)/shard_map/forward_exchange/pallas_call | solution.py:162
  55.2 0.0 copy-start.1
  55.2 1.2 %select_reduce_fusion = f32[768]{0:T(1024)S(1)} fusion(bf16[768,128]{1,0:T(8,128)(2,1)} %get-tuple-element.9, pred[128]{0:T(512)(128)(4,1)S(1)} %iota_compare_fusion.5), kind=kLoop, calls=%fused_computation.31 | loop fusion | flops 294144 | bytes 199808 | tf_op jit(solution)/shard_map/reduce_sum | solution.py:347
  56.5 0.0 copy-done
  56.5 2.9 %fusion.2 = f32[768,256]{0,1:T(8,128)S(1)} fusion(bf16[768,2048]{1,0:T(8,128)(2,1)} %get-tuple-element.11, bf16[1,2048,256]{2,1,0:T(8,128)(2,1)S(1)} %copy-done), kind=kOutput, calls=%fused_computation.7 | convolution fusion | flops 805306368 | bytes 4980736 | tf_op jit(solution)/shard_map/dot_general | solution.py:351
  59.4 0.0 copy-done.2
  59.4 0.0 copy-done.1
  59.4 0.0 copy-start.6
  59.4 0.0 copy-start.7
  59.4 1.1 %fusion.5 = f32[768,256]{0,1:T(8,128)S(1)} fusion(bf16[768,2048]{1,0:T(8,128)(2,1)S(1)} %copy-done.1, bf16[1,2048,256]{2,1,0:T(8,128)(2,1)S(1)} %copy-done.2), kind=kOutput, calls=%fused_computation.10 | convolution fusion | flops 805306368 | bytes 4980736 | tf_op jit(solution)/shard_map/dot_general | solution.py:352
  60.5 0.8 copy-done.6
  61.3 0.3 copy-done.7
  61.6 1.4 %multiply_reduce_fusion = (bf16[768]{0:T(1024)(128)(2,1)S(1)}, bf16[768,256]{0,1:T(8,128)(2,1)S(1)}, bf16[768,256]{0,1:T(8,128)(2,1)S(1)}) fusion(f32[768,256]{0,1:T(8,128)S(1)} %fusion.5, f32[768,256]{0,1:T(8,128)S(1)} %fusion.2, f32[768]{0:T(1024)S(1)} %select_reduce_fusion, bf16[768,2048]{1,0:T(8,128)(2,1)S(1)} %copy-done.6, ...), kind=kOutput, calls=%fused_computation.17 | convolution fusion | flops 808647936 | bytes 6558208 | tf_op jit(solution)/shard_map/dot_general | solution.py:353
  63.0 2.4 %convolution_bitcast_fusion = f32[1,256,2048]{2,1,0:T(8,128)} fusion(bf16[768,2048]{1,0:T(8,128)(2,1)S(1)} %copy-done.6, f32[768]{0:T(1024)S(1)} %select_reduce_fusion, f32[768,256]{0,1:T(8,128)S(1)} %fusion.5, f32[768,256]{0,1:T(8,128)S(1)} %fusion.2), kind=kOutput, calls=%fused_computation.2 | convolution fusion | flops 806682624 | bytes 6818816 | tf_op jit(solution)/shard_map/dot_general | solution.py:385
  65.4 2.4 %convolution_bitcast_fusion.2 = f32[1,2048,256]{2,1,0:T(8,128)} fusion(bf16[768,2048]{1,0:T(8,128)(2,1)S(1)} %copy-done.1, bf16[768,256]{0,1:T(8,128)(2,1)S(1)} %get-tuple-element.13), kind=kOutput, calls=%fused_computation.4 | convolution fusion | flops 805306368 | bytes 5636096 | tf_op jit(solution)/shard_map/dot_general | solution.py:379
  67.8 2.4 %convolution_bitcast_fusion.1 = f32[1,2048,256]{2,1,0:T(8,128)} fusion(bf16[768,2048]{1,0:T(8,128)(2,1)S(1)} %copy-done.1, bf16[768,256]{0,1:T(8,128)(2,1)S(1)} %get-tuple-element.14), kind=kOutput, calls=%fused_computation.3 | convolution fusion | flops 805306368 | bytes 5636096 | tf_op jit(solution)/shard_map/dot_general | solution.py:382
  70.2 1.0 fusion
  71.2 1.0 add_convert_fusion
  72.3 1.1 %slice_dynamic-update-slice_fusion.1 = bf16[768,2304]{1,0:T(8,128)(2,1)} fusion(bf16[768,2048]{1,0:T(8,128)(2,1)S(1)} %add_convert_fusion), kind=kLoop, calls=%fused_computation.15 | loop fusion | bytes 1966080
  73.4 1.1 %slice_dynamic-update-slice_fusion = bf16[768,2304]{1,0:T(8,128)(2,1)} fusion(bf16[768,2304]{1,0:T(8,128)(2,1)} %slice_dynamic-update-slice_fusion.1, bf16[768,2048]{1,0:T(8,128)(2,1)S(1)} %add_convert_fusion), kind=kLoop, calls=%fused_computation.14 | loop fusion | bytes 1966080
  74.5 0.9 slice_dynamic-update-slice_fusion.3
  75.4 0.9 fusion.17
  76.3 0.9 slice_dynamic-update-slice_fusion.2
  77.2 0.9 fusion.18.part
  78.1 0.0 copy-start.3
  78.1 0.0 copy-start.4
  78.1 0.0 copy-start.5
  78.1 26.1 %return_exchange.1 = bf16[192,1152]{1,0:T(8,128)(2,1)} custom-call(bf16[768,2304]{1,0:T(8,128)(2,1)} %fusion.18.part), custom_call_target="tpu_custom_call" | custom-call | tf_op jit(solution)/shard_map/return_exchange/pallas_call | solution.py:289
  104.2 1.3 %fusion.20 = f32[128,1152]{1,0:T(8,128)S(1)} fusion(bf16[192,1152]{1,0:T(8,128)(2,1)} %return_exchange.1, s32[128]{0:T(128)S(1)} %multiply_add_fusion), kind=kOutput, calls=%fused_computation.39 | convolution fusion | flops 56647680 | bytes 1032704 | tf_op jit(solution)/shard_map/dot_general | solution.py:388
  105.6 0.8 slice.43
  106.4 0.0 copy-done.3
  106.4 0.2 select_reduce_fusion.1
  106.6 0.0 copy-done.4
  106.6 0.0 copy-done.5
  106.6 1.1 %convert_multiply_fusion = (f32[128,2]{0,1:T(2,128)}, f32[128]{0:T(128)}) fusion(f32[128]{0:T(128)S(1)} %copy-done.5, bf16[128,2]{0,1:T(2,128)(2,1)S(1)} %select_reduce_fusion.1, f32[128,2]{0,1:T(2,128)S(1)} %copy-done.4), kind=kLoop, calls=%fused_computation.46 | loop fusion | flops 896 | bytes 3584 | tf_op jit(solution)/shard_map/mul | solution.py:393
  (2 shorter events, 0.0 us)
Async XLA Ops:
  0.6 55.8 %copy-start = (bf16[1,2048,256]{2,1,0:T(8,128)(2,1)S(1)}, bf16[1,2048,256]{2,1,0:T(8,128)(2,1)}, u32[]{:S(2)}) copy-start(bf16[1,2048,256]{2,1,0:T(8,128)(2,1)} %param.15) | copy-start | bytes 3145732
  6.9 52.5 %copy-start.2 = (bf16[1,2048,256]{2,1,0:T(8,128)(2,1)S(1)}, bf16[1,2048,256]{2,1,0:T(8,128)(2,1)}, u32[]{:S(2)}) copy-start(bf16[1,2048,256]{2,1,0:T(8,128)(2,1)} %param.16) | copy-start | bytes 3145732
  55.2 4.2 %copy-start.1 = (bf16[768,2048]{1,0:T(8,128)(2,1)S(1)}, bf16[768,2048]{1,0:T(8,128)(2,1)}, u32[]{:S(2)}) copy-start(bf16[768,2048]{1,0:T(8,128)(2,1)} %get-tuple-element.11) | copy-start | bytes 9437188
  59.4 1.9 %copy-start.6 = (bf16[768,2048]{1,0:T(8,128)(2,1)S(1)}, bf16[768,2048]{1,0:T(8,128)(2,1)}, u32[]{:S(2)}) copy-start(bf16[768,2048]{1,0:T(8,128)(2,1)} %get-tuple-element.10) | copy-start | bytes 9437188
  59.4 2.2 %copy-start.7 = (bf16[1,256,2048]{2,1,0:T(8,128)(2,1)S(1)}, bf16[1,256,2048]{2,1,0:T(8,128)(2,1)}, u32[]{:S(2)}) copy-start(bf16[1,256,2048]{2,1,0:T(8,128)(2,1)} %param.17) | copy-start | bytes 3145732
  78.1 28.3 %copy-start.3 = (s32[128,2]{0,1:T(2,128)S(1)}, s32[128,2]{0,1:T(2,128)}, u32[]{:S(2)}) copy-start(s32[128,2]{0,1:T(2,128)} %param.14) | copy-start | bytes 3076
  78.1 28.5 %copy-start.4 = (f32[128,2]{0,1:T(2,128)S(1)}, f32[128,2]{0,1:T(2,128)}, u32[]{:S(2)}) copy-start(f32[128,2]{0,1:T(2,128)} %param.12) | copy-start | bytes 3076
  78.1 28.5 %copy-start.5 = (f32[128]{0:T(128)S(1)}, f32[128]{0:T(128)}, u32[]{:S(2)}) copy-start(f32[128]{0:T(128)} %param.11) | copy-start | bytes 1540
